TPU v7x, 32 devices: a whole 2x2x4 slice. The times are simulated.
32 devices in a mesh: kv: 8 (over z, y), tp: 4 (over x, core).
Axes of the slice: x: 2, y: 2, z: 4, core: 2. Of those that a mesh axis runs over, the one named last changes fastest.
Arguments:
- tokens: bfloat16 [128, 4096], P('kv'), may hold values from -6 to 6
- dec_tokens: bfloat16 [8, 4096], P('kv'), may hold values from -6 to 6
- norm_gain: float32 [4096], replicated, may hold values from 0.1 to 1.9
- w_query: bfloat16 [2, 4096, 1024], P(None, None, 'tp'), may hold values from -0.09375 to 0.09375
- w_key: bfloat16 [2, 4096, 1024], P(None, None, 'tp'), may hold values from -0.15625 to 0.15625
- w_value: bfloat16 [4096, 2048], P(None, 'tp'), may hold values from -0.09375 to 0.09375
- w_out: bfloat16 [2048, 4096], P('tp'), may hold values from -0.125 to 0.125
- head_gain: float32 [256], replicated, may hold values from 0.1 to 1.9
- mix_lambda: float32 [8], P('tp'), may hold values from 0.3 to 0.8
- ctx_keys: bfloat16 [2, 8192, 1024], P(None, 'kv', 'tp'), may hold values from -600 to 600
- ctx_values: bfloat16 [8192, 2048], P('kv', 'tp'), may hold values from -6 to 6
- dec_keys: bfloat16 [2, 8, 2048, 1024], P(None, 'kv', None, 'tp'), may hold values from -600 to 600
- dec_values: bfloat16 [8, 2048, 2048], P('kv', None, 'tp'), may hold values from -6 to 6
- dec_len: int32 [8], P('kv'), may hold values from 256 to 2048, as said below
Outputs:
- piece_out: bfloat16 [128, 4096], P('kv', 'tp')
- dec_out: bfloat16 [8, 4096], P('kv', 'tp')
Inputs may be any that keep to these rules, and one draw needn't show every extreme that they name: `dec_len`: some decoding sequence has exactly 2048 cached positions.
All inputs are finite; a program needn't handle non-finite values.
Results may differ from a plain program's by a relative error of at most 0.03.
The roundings to bfloat16 on the way count: a program that leaves them out, or rounds other values in their place, can miss the bound.
Values may be sent and summed in bfloat16 or wider, within the bound.
A program may use at most 64 MiB of HBM per device.

v0:
```python
import functools
import math

import jax
import jax.numpy as jnp
from jax import lax
from jax.experimental import pallas as pl
from jax.experimental.pallas import tpu as pltpu
from jax.sharding import PartitionSpec as P

DH = 128
epsilon = 1e-06
MESH = pl.DeviceIdType.MESH
F32 = jnp.float32
BF16 = jnp.bfloat16
LANES = 128
C_EXP = DH ** (-0.5) * math.log2(math.e)


def dot(a, b):
    return jnp.dot(a, b, preferred_element_type=F32)


def dot_nt(a, b):
    return lax.dot_general(a, b, (((1,), (1,)), ((), ())), preferred_element_type=F32)


def kernel(
    kv, tp,
    tokens, dec_tokens, norm_gain, w_query, w_key, w_value, w_out, head_gain,
    mix_lambda, dec_len, ctx_keys, ctx_values, dec_keys, dec_values,
    out,
    lam_s, len_s, tok_v, dtok_v, gain_v, hgain_v, wq_v, wk_v, wv_v, wo_v,
    ck_v, cv_v, dk_v, dv_v,
    xs, q_all, kown, vown, st_send, st_recv, att_send, att_recv, p_send, p_recv, d_send, d_recv,
    sem_small, sem_q, sem_k, sem_v, sem_o, sem_c, sem_d,
    qs_sem, qr_sem, ss_sem, sr_sem, as_sem, ar_sem, ps_sem, pr_sem, ds_sem, dr_sem,
):
    me = lax.axis_index("kv")
    mt = lax.axis_index("tp")
    rows, width = tokens.shape
    drows = dec_tokens.shape[0]
    w = w_query.shape[2]
    heads = w // DH
    ctx = ctx_keys.shape[1]
    slots = dec_keys.shape[2]
    total = rows * kv
    cols = w_out.shape[1] // tp
    blocks = total // LANES
    padded = xs.shape[0]

    def tp_peer(d):
        chip = lax.rem(mt // 2 + d // 2, tp // 2)
        return chip * 2 + lax.rem(mt + d, 2)

    barrier = pltpu.get_barrier_semaphore()
    for d in range(1, kv):
        pl.semaphore_signal(
            barrier, inc=1, device_id=(lax.rem(me + d, kv), mt), device_id_type=MESH
        )
    for d in range(1, tp):
        pl.semaphore_signal(
            barrier, inc=1, device_id=(me, tp_peer(d)), device_id_type=MESH
        )

    small = [
        pltpu.make_async_copy(tokens, tok_v, sem_small.at[0]),
        pltpu.make_async_copy(dec_tokens, dtok_v, sem_small.at[1]),
        pltpu.make_async_copy(norm_gain, gain_v, sem_small.at[2]),
        pltpu.make_async_copy(head_gain, hgain_v, sem_small.at[3]),
        pltpu.make_async_copy(mix_lambda, lam_s, sem_small.at[4]),
        pltpu.make_async_copy(dec_len, len_s, sem_small.at[5]),
    ]
    for c in small:
        c.start()

    def weight_copies(src, dst, sem, parts):
        step = width // parts
        out = []
        for c in range(2):
            row = []
            for i in range(parts):
                sl = pl.ds(i * step, step)
                row.append(
                    pltpu.make_async_copy(src.at[c, sl], dst.at[c, sl], sem.at[c * parts + i])
                )
            out.append(row)
        return out

    parts = 2
    q_copies = weight_copies(w_query, wq_v, sem_q, parts)
    k_copies = weight_copies(w_key, wk_v, sem_k, parts)
    vstep = width // 4
    v_copies = [
        pltpu.make_async_copy(
            w_value.at[pl.ds(i * vstep, vstep)], wv_v.at[pl.ds(i * vstep, vstep)], sem_v.at[i]
        )
        for i in range(4)
    ]
    ck_copies = [pltpu.make_async_copy(ctx_keys.at[c], ck_v.at[c], sem_c.at[c]) for c in range(2)]
    cv_copy = pltpu.make_async_copy(ctx_values, cv_v, sem_c.at[2])
    dk_copies = [pltpu.make_async_copy(dec_keys.at[c], dk_v.at[c], sem_d.at[c]) for c in range(2)]
    dv_copy = pltpu.make_async_copy(dec_values, dv_v, sem_d.at[2])
    wo_copies = []
    for d in range(tp):
        start = pl.multiple_of(tp_peer(d) * cols, LANES)
        wo_copies.append(
            pltpu.make_async_copy(w_out.at[:, pl.ds(start, cols)], wo_v.at[d], sem_o.at[d])
        )
    k_flat = [c for row in k_copies for c in row]
    stages = [
        [c for row in q_copies for c in row],
        k_flat,
        v_copies,
        ck_copies + [cv_copy],
        dk_copies + [dv_copy],
        wo_copies,
    ]

    def start_stage(i):
        for c in stages[i]:
            c.start()

    start_stage(0)

    kown[...] = jnp.zeros_like(kown)
    vown[...] = jnp.zeros_like(vown)
    xs[rows:, :] = jnp.zeros((padded - rows, width), BF16)
    for c in small:
        c.wait()
    gain = gain_v[...]

    def normed(x):
        xf = x.astype(F32)
        inv = lax.rsqrt(jnp.mean(xf * xf, axis=-1, keepdims=True) + epsilon)
        return (xf * inv * gain).astype(BF16)

    xs[0:rows, :] = normed(tok_v[...])
    xs[rows : rows + drows, :] = normed(dtok_v[...])

    def project(copies, weights, c):
        step = width // parts
        acc = None
        for i in range(parts):
            copies[c][i].wait()
            term = dot(xs[:, i * step : (i + 1) * step], weights[c, i * step : (i + 1) * step, :])
            acc = term if acc is None else acc + term
        return acc.astype(BF16)

    dec_q = []
    for c in range(2):
        qc = project(q_copies, wq_v, c)
        q_all[me, :, c * w : (c + 1) * w] = qc[0:rows]
        dec_q.append(qc[rows:])
        start_stage(1 + c)
        if c == 1:
            start_stage(3)
    pl.semaphore_wait(barrier, kv + tp - 2)

    def to_kv(src, dst, send, recv, d):
        return pltpu.make_async_remote_copy(
            src_ref=src, dst_ref=dst, send_sem=send.at[d], recv_sem=recv.at[d],
            device_id=(lax.rem(me + d, kv), mt), device_id_type=MESH,
        )

    far_first = sorted(range(1, kv), key=lambda d: (-min(d, kv - d), d))
    q_sends = [to_kv(q_all.at[me], q_all.at[me], qs_sem, qr_sem, d) for d in far_first]
    for c in q_sends:
        c.start()

    dec_k = []
    for c in range(2):
        kc = project(k_copies, wk_v, c)
        kown[c, 0:rows, :] = kc[0:rows]
        dec_k.append(kc[rows:])
        start_stage(4 + c)
    acc = None
    for i in range(4):
        v_copies[i].wait()
        term = dot(xs[:, i * vstep : (i + 1) * vstep], wv_v[i * vstep : (i + 1) * vstep, :])
        acc = term if acc is None else acc + term
    vc = acc.astype(BF16)
    vown[0:rows, :] = vc[0:rows]
    dec_v = vc[rows:]

    for c in ck_copies:
        c.wait()
    cv_copy.wait()
    for c in q_sends:
        c.wait_recv()
    vw = 2 * DH
    nstat = 2 * heads
    per = LANES // rows

    def head_block(h, b):
        slots_b = pl.ds(b * per, per)
        qb = q_all[slots_b].reshape(LANES, 2 * w)
        pos = b * LANES + lax.broadcasted_iota(jnp.int32, (LANES, LANES), 0)
        lane = lax.broadcasted_iota(jnp.int32, (LANES, LANES), 1)
        ok = (lane < rows) & (lane + me * rows <= pos)
        if h == 0:
            stats = jnp.zeros((LANES, LANES), F32)
        else:
            stats = st_send[slots_b].reshape(LANES, LANES)
        hs = slice(h * DH, (h + 1) * DH)
        hv = slice(h * vw, (h + 1) * vw)
        for c in range(2):
            q = qb[:, c * w + h * DH : c * w + (h + 1) * DH]
            far = dot_nt(q, ck_v[c, :, hs])
            near = dot_nt(q, kown[c, :, hs])
            near = jnp.where(ok, near, -jnp.inf)
            top = jnp.maximum(
                jnp.max(far, axis=-1, keepdims=True), jnp.max(near, axis=-1, keepdims=True)
            )
            ef = jnp.exp2((far - top) * C_EXP)
            en = jnp.exp2((near - top) * C_EXP)
            tot = jnp.sum(ef, axis=-1, keepdims=True) + jnp.sum(en, axis=-1, keepdims=True)
            att = dot(ef.astype(BF16), cv_v[:, hv]) + dot(en.astype(BF16), vown[:, hv])
            att_send[h, slots_b, :, c * vw : (c + 1) * vw] = att.astype(BF16).reshape(
                per, rows, vw
            )
            i = 2 * h + c
            stats = jnp.where(lane == i, top, stats)
            stats = jnp.where(lane == nstat + i, tot, stats)
        st_send[slots_b] = stats.reshape(per, rows, LANES)

    a_sends = []
    for h in range(heads):
        if blocks == 1:
            head_block(h, 0)
        else:
            pl.loop(0, blocks)(functools.partial(head_block, h))
        if h == heads - 1:
            st_sends = []
            for d in far_first:
                peer = lax.rem(me + d, kv)
                st_sends.append(to_kv(st_send.at[peer], st_recv.at[me], ss_sem, sr_sem, d))
                st_sends[-1].start()
        a_sends.append({})
        for d in far_first:
            peer = lax.rem(me + d, kv)
            a_sends[h][d] = to_kv(
                att_send.at[h, peer], att_recv.at[h, me], as_sem.at[h], ar_sem.at[h], d
            )
            a_sends[h][d].start()

    hgain = hgain_v[...]
    group = 16
    hrow = lax.broadcasted_iota(jnp.int32, (group, w), 0)
    hcol = lax.broadcasted_iota(jnp.int32, (group, w), 1) // DH
    own_head = hrow == hcol
    row1 = lax.broadcasted_iota(jnp.int32, (group, 1), 0)
    lam_col = jnp.zeros((group, 1), F32)
    for h in range(heads):
        lam_col = jnp.where(row1 == h, lam_s[h], lam_col)
    for c in dk_copies:
        c.wait()
    slot_id = lax.broadcasted_iota(jnp.int32, (group, slots), 1)
    vrow = lax.broadcasted_iota(jnp.int32, (group, heads * vw), 0)
    vcol = lax.broadcasted_iota(jnp.int32, (group, heads * vw), 1) // vw
    dec_att = []
    for r in range(drows):
        far_p = []
        near_p = []
        for c in range(2):
            qr = jnp.broadcast_to(dec_q[c][r : r + 1].astype(F32), (group, w))
            qr = jnp.where(own_head, qr, 0.0)
            kr = dec_k[c][r : r + 1].astype(F32)
            near = jnp.sum(qr * kr, axis=-1, keepdims=True)
            far = dot_nt(qr.astype(BF16), dk_v[c, r])
            far = jnp.where(slot_id < len_s[r], far, -jnp.inf)
            top = jnp.maximum(jnp.max(far, axis=-1, keepdims=True), near)
            ef = jnp.exp2((far - top) * C_EXP)
            en = jnp.exp2((near - top) * C_EXP)
            den = jnp.sum(ef, axis=-1, keepdims=True) + en
            far_p.append(ef / den)
            near_p.append(en / den)
        far_w = (far_p[0] - lam_col * far_p[1]).astype(BF16)
        near_w = (near_p[0] - lam_col * near_p[1]).astype(BF16).astype(F32)
        if r == 0:
            dv_copy.wait()
        att = dot(far_w, dv_v[r]) + near_w * dec_v[r : r + 1].astype(F32)
        dec_att.append(jnp.sum(jnp.where(vrow == vcol, att, 0.0), axis=0, keepdims=True))

    def head_norm(att, h):
        inv = lax.rsqrt(jnp.mean(att * att, axis=-1, keepdims=True) + epsilon)
        return (att * inv * hgain).astype(BF16)

    def out_project(ho, d):
        acc = None
        for h in range(heads):
            term = dot(ho[h], wo_v[d, h * vw : (h + 1) * vw, :])
            acc = term if acc is None else acc + term
        return acc.astype(BF16)

    def to_tp(src, dst, send, recv, d):
        return pltpu.make_async_remote_copy(
            src_ref=src.at[d], dst_ref=dst.at[d], send_sem=send.at[d], recv_sem=recv.at[d],
            device_id=(me, tp_peer(d)), device_id_type=MESH,
        )

    dec_rows = jnp.concatenate(dec_att, axis=0) if drows > 1 else dec_att[0]
    dec_rows = dec_rows if drows > 1 else jnp.broadcast_to(dec_rows, (group, heads * vw))
    dec_ho = [head_norm(dec_rows[:, h * vw : (h + 1) * vw], h) for h in range(heads)]
    for c in wo_copies:
        c.wait()
    order = list(range(tp - 1, 0, -1))
    d_sends = {d: to_tp(d_send, d_recv, ds_sem, dr_sem, d) for d in order}
    for d in order:
        d_send[d] = out_project(dec_ho, d)[0:drows]
        d_sends[d].start()
    dec_own = out_project(dec_ho, 0)[0:drows]

    for c in st_sends:
        c.wait_recv()
    lane = lax.broadcasted_iota(jnp.int32, (rows, LANES), 1)
    sts = {0: st_send[me]}
    for d in range(1, kv):
        sts[d] = st_recv[lax.rem(me - d + kv, kv)]
    top = sts[0]
    for d in range(1, kv):
        top = jnp.maximum(top, sts[d])
    den = jnp.zeros((rows, LANES), F32)
    fac = {}
    for d in range(kv):
        fac[d] = jnp.exp2((sts[d] - top) * C_EXP)
        den = den + fac[d] * pltpu.roll(sts[d], LANES - nstat, 1)
    den = jnp.where(lane < nstat, den, 1.0)
    part = jnp.ones((rows, LANES), F32)
    for h in range(heads):
        part = jnp.where(lane == 2 * h + 1, -lam_s[h], part)
    part = part / den
    for d in range(kv):
        fac[d] = fac[d] * part
    ho = []
    for h in range(heads):
        total_att = None
        for d in range(kv):
            if d == 0:
                blk = att_send[h, me]
            else:
                a_sends[h][d].wait_recv()
                blk = att_recv[h, lax.rem(me - d + kv, kv)]
            for c in range(2):
                i = 2 * h + c
                term = fac[d][:, i : i + 1] * blk[:, c * vw : (c + 1) * vw].astype(F32)
                total_att = term if total_att is None else total_att + term
        ho.append(head_norm(total_att, h))

    p_sends = {d: to_tp(p_send, p_recv, ps_sem, pr_sem, d) for d in order}
    for d in order:
        p_send[d] = out_project(ho, d)
        p_sends[d].start()
    own = out_project(ho, 0).astype(F32)
    dsum = dec_own.astype(F32)
    for d in order:
        d_sends[d].wait_recv()
        dsum = dsum + d_recv[d].astype(F32)
    out[rows:, :] = jnp.broadcast_to(dsum, (out.shape[0] - rows, cols)).astype(BF16) if (
        drows == 1
    ) else jnp.concatenate(
        [dsum, jnp.zeros((out.shape[0] - rows - drows, cols), F32)], axis=0
    ).astype(BF16)
    for d in order:
        p_sends[d].wait_recv()
        own = own + p_recv[d].astype(F32)
    out[0:rows, :] = own.astype(BF16)
    for c in q_sends + st_sends + [c for row in a_sends for c in row.values()]:
        c.wait_send()
    for d in order:
        d_sends[d].wait_send()
        p_sends[d].wait_send()


def body(
    tokens, dec_tokens, norm_gain, w_query, w_key, w_value, w_out, head_gain, mix_lambda,
    ctx_keys, ctx_values, dec_keys, dec_values, dec_len, *, kv, tp,
):
    rows, width = tokens.shape
    drows = dec_tokens.shape[0]
    w = w_query.shape[2]
    heads = w // DH
    vwid = w_value.shape[1]
    ctx = ctx_keys.shape[1]
    slots = dec_keys.shape[2]
    cols = w_out.shape[1] // tp
    padded = rows + -(-drows // 16) * 16
    any_spec = pl.BlockSpec(memory_space=pltpu.HBM)
    vmem = pl.BlockSpec(memory_space=pltpu.VMEM)
    dma = pltpu.SemaphoreType.DMA
    V = pltpu.VMEM
    out = pl.pallas_call(
        functools.partial(kernel, kv, tp),
        out_shape=jax.ShapeDtypeStruct((padded, cols), BF16),
        in_specs=[any_spec] * 14,
        out_specs=vmem,
        scratch_shapes=[
            pltpu.SMEM((heads,), F32), pltpu.SMEM((drows,), jnp.int32),
            V((rows, width), BF16), V((drows, width), BF16), V((1, width), F32),
            V((1, 2 * DH), F32),
            V((2, width, w), BF16), V((2, width, w), BF16), V((width, vwid), BF16),
            V((tp, vwid, cols), BF16),
            V((2, ctx, w), BF16), V((ctx, vwid), BF16),
            V((2, drows, slots, w), BF16), V((drows, slots, vwid), BF16),
            V((padded, width), BF16), V((kv, rows, 2 * w), BF16),
            V((2, LANES, w), BF16), V((LANES, vwid), BF16),
            V((kv, rows, LANES), F32), V((kv, rows, LANES), F32),
            V((heads, kv, rows, 4 * DH), BF16), V((heads, kv, rows, 4 * DH), BF16),
            V((tp, rows, cols), BF16), V((tp, rows, cols), BF16),
            V((tp, drows, cols), BF16), V((tp, drows, cols), BF16),
            dma((6,)), dma((4,)), dma((4,)), dma((4,)), dma((tp,)), dma((3,)), dma((3,)),
            dma((kv,)), dma((kv,)), dma((kv,)), dma((kv,)), dma((heads, kv)), dma((heads, kv)),
            dma((tp,)), dma((tp,)), dma((tp,)), dma((tp,)),
        ],
        compiler_params=pltpu.CompilerParams(
            collective_id=0, has_side_effects=True, vmem_limit_bytes=60 * 1024 * 1024
        ),
    )(
        tokens, dec_tokens, norm_gain.reshape(1, width), w_query, w_key, w_value, w_out,
        head_gain.reshape(1, 2 * DH), mix_lambda, dec_len, ctx_keys, ctx_values, dec_keys,
        dec_values,
    )
    def split(src, piece_ref, dec_ref):
        piece_ref[...] = src[0:rows, :]
        dec_ref[...] = src[rows : rows + drows, :]

    return pl.pallas_call(
        split,
        out_shape=(
            jax.ShapeDtypeStruct((rows, cols), BF16),
            jax.ShapeDtypeStruct((drows, cols), BF16),
        ),
        in_specs=[vmem],
        out_specs=(vmem, vmem),
    )(out)


def solution(mesh):
    in_specs = (
        P("kv", None),
        P("kv", None),
        P(),
        P(None, None, "tp"),
        P(None, None, "tp"),
        P(None, "tp"),
        P("tp", None),
        P(),
        P("tp"),
        P(None, "kv", "tp"),
        P("kv", "tp"),
        P(None, "kv", None, "tp"),
        P("kv", None, "tp"),
        P("kv"),
    )
    out_specs = (P("kv", "tp"), P("kv", "tp"))
    step = functools.partial(body, kv=mesh.shape["kv"], tp=mesh.shape["tp"])
    return jax.shard_map(step, mesh=mesh, in_specs=in_specs, out_specs=out_specs, check_vma=False)
```

profile of v0, /device:TPU:0, one launch (start us, length us, event | category | flops | bytes accessed | tf_op | source)
XLA Modules:
  0.0 29.1 jit_solution(5396678087312868934)
XLA Ops:
  1.3 26.3 %shard_map.149.src = bf16[32,1024]{1,0:T(8,128)(2,1)} custom-call(bf16[16,4096]{1,0:T(8,128)(2,1)} %tokens.1, bf16[1,4096]{1,0:T(2,128)(2,1)} %dec_tokens.1, f32[1,4096]{1,0:T(1,128)} %bitcast.2, bf16[2,4096,256]{2,1,0:T(8,128)(2,1)} %w_query.1, bf16[2,4096,256]{2,1,0:T(8,128)(2,1)} %w_key.1, bf16[4096,512]{1,0:T(8,128)(2,1)} %w_value.1, ...), custom_call_target="tpu_custom_call" | custom-call | tf_op jit(solution)/shard_map/pallas_call | solution.py:392
  27.6 1.5 %shard_map.150 = (bf16[16,1024]{1,0:T(8,128)(2,1)}, bf16[1,1024]{1,0:T(2,128)(2,1)}) custom-call(bf16[32,1024]{1,0:T(8,128)(2,1)} %shard_map.149.src), custom_call_target="tpu_custom_call" | custom-call | tf_op jit(solution)/shard_map/pallas_call | solution.py:427
where the time goes:
time: 29.2 us; the launch traced here: 29.1 us
  Pallas kernels  27.8 us (95%)
  between operations  1.29 us (4%)
    pallas_call x1, Pallas kernels, body(): pl.pallas_call(functools.partial(kernel, kv, tp), out_shape=jax.ShapeDtyp...  26.3 us
    pallas_call x1, Pallas kernels, body(): pl.pallas_call(split, out_shape=(jax.ShapeDtypeStruct((rows, cols), BF16)...  1.46 us

commit v1 on v0

v1 whole, which is shorter than its diff:
```python
import functools
import math

import jax
import jax.numpy as jnp
from jax import lax
from jax.experimental import pallas as pl
from jax.experimental.pallas import tpu as pltpu
from jax.sharding import PartitionSpec as P

DH = 128
epsilon = 1e-06
MESH = pl.DeviceIdType.MESH
F32 = jnp.float32
BF16 = jnp.bfloat16
LANES = 128
C_EXP = DH ** (-0.5) * math.log2(math.e)
Q_PARTS = 4
K_PARTS = 2
V_PARTS = 4


def dot(a, b):
    return jnp.dot(a, b, preferred_element_type=F32)


def dot_nt(a, b):
    return lax.dot_general(a, b, (((1,), (1,)), ((), ())), preferred_element_type=F32)


def kernel(
    kv, tp,
    tokens, dec_tokens, norm_gain, w_query, w_key, w_value, w_out, head_gain,
    mix_lambda, dec_len, ctx_keys, ctx_values, dec_keys, dec_values,
    out,
    lam_s, len_s, tok_v, dtok_v, gain_v, hgain_v, wq_v, wk_v, wv_v, wo_v,
    ck_v, cv_v, dk_v, dv_v,
    xs, q_all, kown, vown, st_send, st_recv, att_send, att_recv, po_acc, p_send, p_recv,
    d_send, d_recv,
    sem_small, sem_q, sem_k, sem_v, sem_o, sem_c, sem_d,
    qs_sem, qr_sem, ss_sem, sr_sem, as_sem, ar_sem, ps_sem, pr_sem, ds_sem, dr_sem,
):
    me = lax.axis_index("kv")
    mt = lax.axis_index("tp")
    rows, width = tokens.shape
    drows = dec_tokens.shape[0]
    w = w_query.shape[2]
    heads = w // DH
    vw = 2 * DH
    slots = dec_keys.shape[2]
    total = rows * kv
    cols = w_out.shape[1] // tp
    blocks = total // LANES
    padded = xs.shape[0]
    per = LANES // rows

    def tp_peer(d):
        chip = lax.rem(mt // 2 + d // 2, tp // 2)
        return chip * 2 + lax.rem(mt + d, 2)

    barrier = pltpu.get_barrier_semaphore()
    for d in range(1, kv):
        pl.semaphore_signal(
            barrier, inc=1, device_id=(lax.rem(me + d, kv), mt), device_id_type=MESH
        )
    for d in range(1, tp):
        pl.semaphore_signal(
            barrier, inc=1, device_id=(me, tp_peer(d)), device_id_type=MESH
        )

    small = [
        pltpu.make_async_copy(tokens, tok_v, sem_small.at[0]),
        pltpu.make_async_copy(dec_tokens, dtok_v, sem_small.at[1]),
        pltpu.make_async_copy(norm_gain, gain_v, sem_small.at[2]),
        pltpu.make_async_copy(head_gain, hgain_v, sem_small.at[3]),
        pltpu.make_async_copy(mix_lambda, lam_s, sem_small.at[4]),
        pltpu.make_async_copy(dec_len, len_s, sem_small.at[5]),
    ]
    for c in small:
        c.start()

    qstep = width // Q_PARTS
    kstep = width // K_PARTS
    vstep = width // V_PARTS
    q_copies = []
    for h in range(heads):
        q_copies.append([])
        for i in range(Q_PARTS):
            sl = (slice(None), pl.ds(i * qstep, qstep), pl.ds(h * DH, DH))
            q_copies[h].append(
                pltpu.make_async_copy(
                    w_query.at[sl], wq_v.at[sl], sem_q.at[h * Q_PARTS + i]
                )
            )
    k_copies = []
    for i in range(K_PARTS):
        sl = (slice(None), pl.ds(i * kstep, kstep))
        k_copies.append(pltpu.make_async_copy(w_key.at[sl], wk_v.at[sl], sem_k.at[i]))
    v_copies = [
        pltpu.make_async_copy(
            w_value.at[pl.ds(i * vstep, vstep)], wv_v.at[pl.ds(i * vstep, vstep)], sem_v.at[i]
        )
        for i in range(V_PARTS)
    ]
    ck_copy = pltpu.make_async_copy(ctx_keys, ck_v, sem_c.at[0])
    cv_copy = pltpu.make_async_copy(ctx_values, cv_v, sem_c.at[1])
    dk_copy = pltpu.make_async_copy(dec_keys, dk_v, sem_d.at[0])
    dv_copy = pltpu.make_async_copy(dec_values, dv_v, sem_d.at[1])
    wo_copies = []
    for d in range(tp):
        start = pl.multiple_of(tp_peer(d) * cols, LANES)
        wo_copies.append(
            pltpu.make_async_copy(w_out.at[:, pl.ds(start, cols)], wo_v.at[d], sem_o.at[d])
        )
    for row in q_copies:
        for c in row:
            c.start()

    kown[...] = jnp.zeros_like(kown)
    vown[...] = jnp.zeros_like(vown)
    xs[rows:, :] = jnp.zeros((padded - rows, width), BF16)
    for c in small:
        c.wait()
    gain = gain_v[...]

    def normed(x):
        xf = x.astype(F32)
        inv = lax.rsqrt(jnp.mean(xf * xf, axis=-1, keepdims=True) + epsilon)
        return (xf * inv * gain).astype(BF16)

    xs[0:rows, :] = normed(tok_v[...])
    xs[rows : rows + drows, :] = normed(dtok_v[...])

    def to_kv(src, dst, send, recv, d):
        return pltpu.make_async_remote_copy(
            src_ref=src, dst_ref=dst, send_sem=send, recv_sem=recv,
            device_id=(lax.rem(me + d, kv), mt), device_id_type=MESH,
        )

    far_first = sorted(range(1, kv), key=lambda d: (-min(d, kv - d), d))
    dec_qh = []
    q_sends = []
    for h in range(heads):
        hs = slice(h * DH, (h + 1) * DH)
        acc = None
        for i in range(Q_PARTS):
            q_copies[h][i].wait()
            sl = slice(i * qstep, (i + 1) * qstep)
            wt = jnp.concatenate([wq_v[0, sl, hs], wq_v[1, sl, hs]], axis=1)
            term = dot(xs[:, sl], wt)
            acc = term if acc is None else acc + term
        qh = acc.astype(BF16)
        q_all[h, me] = qh[0:rows]
        dec_qh.append(qh[rows:])
        if h == 0:
            for c in k_copies + [ck_copy]:
                c.start()
        if h == heads - 1:
            for c in v_copies + [cv_copy]:
                c.start()
        if h == 0:
            pl.semaphore_wait(barrier, kv + tp - 2)
        q_sends.append(
            {
                d: to_kv(q_all.at[h, me], q_all.at[h, me], qs_sem.at[h, d], qr_sem.at[h, d], d)
                for d in far_first
            }
        )
        for d in far_first:
            q_sends[h][d].start()

    acc = [None, None]
    for i in range(K_PARTS):
        k_copies[i].wait()
        sl = slice(i * kstep, (i + 1) * kstep)
        for c in range(2):
            term = dot(xs[:, sl], wk_v[c, sl, :])
            acc[c] = term if acc[c] is None else acc[c] + term
    dec_k = []
    for c in range(2):
        kc = acc[c].astype(BF16)
        kown[c, 0:rows, :] = kc[0:rows]
        dec_k.append(kc[rows:])
    for c in [dk_copy, dv_copy]:
        c.start()
    acc = None
    for i in range(V_PARTS):
        v_copies[i].wait()
        term = dot(xs[:, i * vstep : (i + 1) * vstep], wv_v[i * vstep : (i + 1) * vstep, :])
        acc = term if acc is None else acc + term
    vc = acc.astype(BF16)
    vown[0:rows, :] = vc[0:rows]
    dec_v = vc[rows:]
    for c in wo_copies:
        c.start()

    ck_copy.wait()
    cv_copy.wait()
    nstat = 4

    def head_block(h, b):
        slots_b = pl.ds(b * per, per)
        qb = q_all[h, slots_b].reshape(LANES, 2 * DH)
        pos = b * LANES + lax.broadcasted_iota(jnp.int32, (LANES, LANES), 0)
        lane = lax.broadcasted_iota(jnp.int32, (LANES, LANES), 1)
        ok = (lane < rows) & (lane + me * rows <= pos)
        stats = jnp.zeros((LANES, LANES), F32)
        hs = slice(h * DH, (h + 1) * DH)
        hv = slice(h * vw, (h + 1) * vw)
        far_p = []
        near_p = []
        for c in range(2):
            q = qb[:, c * DH : (c + 1) * DH]
            far = dot_nt(q, ck_v[c, :, hs])
            near = dot_nt(q, kown[c, :, hs])
            near = jnp.where(ok, near, -jnp.inf)
            top = jnp.maximum(
                jnp.max(far, axis=-1, keepdims=True), jnp.max(near, axis=-1, keepdims=True)
            )
            ef = jnp.exp2((far - top) * C_EXP)
            en = jnp.exp2((near - top) * C_EXP)
            tot = jnp.sum(ef, axis=-1, keepdims=True) + jnp.sum(en, axis=-1, keepdims=True)
            far_p.append(ef.astype(BF16))
            near_p.append(en.astype(BF16))
            stats = jnp.where(lane == c, top, stats)
            stats = jnp.where(lane == 2 + c, tot, stats)
        for c in range(2):
            att = dot(far_p[c], cv_v[:, hv]) + dot(near_p[c], vown[:, hv])
            att_send[h, slots_b, :, c * vw : (c + 1) * vw] = att.astype(BF16).reshape(
                per, rows, vw
            )
        by_row = jnp.transpose(stats)
        lane8 = lax.broadcasted_iota(jnp.int32, (per, LANES), 1) // rows
        packed = jnp.zeros((per, LANES), F32)
        for s in range(nstat):
            line = jnp.broadcast_to(by_row[s : s + 1, :], (per, LANES))
            line = pltpu.roll(line, rows, 1, stride=rows, stride_axis=0)
            if s:
                line = pltpu.roll(line, s * rows, 1)
            packed = jnp.where(lane8 == s, line, packed)
        for o in range(per):
            st_send[h, b * per + o] = packed[per - 1 - o : per - o, :]

    a_sends = []
    st_sends = []
    for h in range(heads):
        for d in far_first:
            q_sends[h][d].wait_recv()
        if blocks == 1:
            head_block(h, 0)
        else:
            pl.loop(0, blocks)(functools.partial(head_block, h))
        st_recv[h, 0] = st_send[h, me]
        for i in range(kv - 1):
            peer = i + jnp.where(me <= i, 1, 0)
            d = lax.rem(peer - me + kv, kv)
            to_kv(
                st_send.at[h, peer], st_recv.at[h, d], ss_sem.at[h, d], sr_sem.at[h, d], d
            ).start()
        for i in range(kv - 1):
            peer = i + jnp.where(me <= i, 1, 0)
            d = lax.rem(peer - me + kv, kv)
            to_kv(
                att_send.at[h, peer], att_recv.at[h, d], as_sem.at[h, d], ar_sem.at[h, d], d
            ).start()
        st_sends.append({})
        a_sends.append({})
        for d in range(1, kv):
            peer = lax.rem(me + d, kv)
            st_sends[h][d] = to_kv(
                st_send.at[h, peer], st_recv.at[h, d], ss_sem.at[h, d], sr_sem.at[h, d], d
            )
            a_sends[h][d] = to_kv(
                att_send.at[h, peer], att_recv.at[h, d], as_sem.at[h, d], ar_sem.at[h, d], d
            )

    hgain = hgain_v[...]
    group = 16
    hrow = lax.broadcasted_iota(jnp.int32, (group, w), 0)
    hcol = lax.broadcasted_iota(jnp.int32, (group, w), 1) // DH
    own_head = hrow == hcol
    row1 = lax.broadcasted_iota(jnp.int32, (group, 1), 0)
    lam_col = jnp.zeros((group, 1), F32)
    for h in range(heads):
        lam_col = jnp.where(row1 == h, lam_s[h], lam_col)
    dk_copy.wait()
    slot_id = lax.broadcasted_iota(jnp.int32, (group, slots), 1)
    vrow = lax.broadcasted_iota(jnp.int32, (group, heads * vw), 0)
    vcol = lax.broadcasted_iota(jnp.int32, (group, heads * vw), 1) // vw
    dec_q = [
        jnp.concatenate([q[:, c * DH : (c + 1) * DH] for q in dec_qh], axis=1) for c in range(2)
    ]
    dec_att = []
    for r in range(drows):
        far_p = []
        near_p = []
        for c in range(2):
            qr = jnp.broadcast_to(dec_q[c][r : r + 1].astype(F32), (group, w))
            qr = jnp.where(own_head, qr, 0.0)
            kr = dec_k[c][r : r + 1].astype(F32)
            near = jnp.sum(qr * kr, axis=-1, keepdims=True)
            far = dot_nt(qr.astype(BF16), dk_v[c, r])
            far = jnp.where(slot_id < len_s[r], far, -jnp.inf)
            top = jnp.maximum(jnp.max(far, axis=-1, keepdims=True), near)
            ef = jnp.exp2((far - top) * C_EXP)
            en = jnp.exp2((near - top) * C_EXP)
            den = jnp.sum(ef, axis=-1, keepdims=True) + en
            far_p.append(ef / den)
            near_p.append(en / den)
        far_w = (far_p[0] - lam_col * far_p[1]).astype(BF16)
        near_w = (near_p[0] - lam_col * near_p[1]).astype(BF16).astype(F32)
        if r == 0:
            dv_copy.wait()
        att = dot(far_w, dv_v[r]) + near_w * dec_v[r : r + 1].astype(F32)
        dec_att.append(jnp.sum(jnp.where(vrow == vcol, att, 0.0), axis=0, keepdims=True))

    def head_norm(att):
        inv = lax.rsqrt(jnp.mean(att * att, axis=-1, keepdims=True) + epsilon)
        return (att * inv * hgain).astype(BF16)

    def to_tp(src, dst, send, recv, d):
        return pltpu.make_async_remote_copy(
            src_ref=src.at[d], dst_ref=dst.at[d], send_sem=send.at[d], recv_sem=recv.at[d],
            device_id=(me, tp_peer(d)), device_id_type=MESH,
        )

    def out_part(ho, d, h):
        return dot(ho, wo_v[d, h * vw : (h + 1) * vw, :])

    dec_rows = jnp.concatenate(dec_att, axis=0) if drows > 1 else dec_att[0]
    dec_rows = dec_rows if drows > 1 else jnp.broadcast_to(dec_rows, (group, heads * vw))
    dec_ho = [head_norm(dec_rows[:, h * vw : (h + 1) * vw]) for h in range(heads)]
    for c in wo_copies:
        c.wait()
    order = list(range(tp - 1, 0, -1))

    def dec_project(d):
        acc = None
        for h in range(heads):
            term = out_part(dec_ho[h], d, h)
            acc = term if acc is None else acc + term
        return acc[0:drows].astype(BF16)

    d_sends = {d: to_tp(d_send, d_recv, ds_sem, dr_sem, d) for d in order}
    for d in order:
        d_send[d] = dec_project(d)
        d_sends[d].start()
    dec_own = dec_project(0)

    lane = lax.broadcasted_iota(jnp.int32, (1, LANES), 1)
    p_sends = {d: to_tp(p_send, p_recv, ps_sem, pr_sem, d) for d in order}
    own = None
    for h in range(heads):
        for d in range(1, kv):
            st_sends[h][d].wait_recv()
        sts = st_recv[h].reshape(kv, LANES)
        top = jnp.max(sts, axis=0, keepdims=True)
        fac = jnp.exp2((sts - top) * C_EXP)
        den = jnp.sum(fac * pltpu.roll(sts, LANES - 2 * rows, 1), axis=0, keepdims=True)
        den = jnp.where(lane < 2 * rows, den, 1.0)
        part = jnp.where(lane < rows, 1.0, -lam_s[h]) / den
        fac = jnp.transpose(fac * part)
        total_att = None
        for d in [0] + far_first[::-1]:
            if d == 0:
                blk = att_send[h, me]
            else:
                a_sends[h][d].wait_recv()
                blk = att_recv[h, d]
            for c in range(2):
                term = fac[c * rows : (c + 1) * rows, d : d + 1] * blk[
                    :, c * vw : (c + 1) * vw
                ].astype(F32)
                total_att = term if total_att is None else total_att + term
        ho = head_norm(total_att)
        last = h == heads - 1
        for d in order + [0]:
            term = out_part(ho, d, h)
            if h > 0:
                term = term + po_acc[d]
            if not last:
                po_acc[d] = term
            elif d > 0:
                p_send[d] = term.astype(BF16)
                p_sends[d].start()
            else:
                own = term.astype(BF16).astype(F32)
    dsum = dec_own.astype(F32)
    for d in order:
        d_sends[d].wait_recv()
        dsum = dsum + d_recv[d].astype(F32)
    out[rows:, :] = jnp.broadcast_to(dsum, (out.shape[0] - rows, cols)).astype(BF16) if (
        drows == 1
    ) else jnp.concatenate(
        [dsum, jnp.zeros((out.shape[0] - rows - drows, cols), F32)], axis=0
    ).astype(BF16)
    for rem_sends in q_sends + st_sends + a_sends:
        for d in range(1, kv):
            rem_sends[d].wait_send()
    for d in order:
        d_sends[d].wait_send()
    for d in order[::-1]:
        p_sends[d].wait_recv()
        own = own + p_recv[d].astype(F32)
    out[0:rows, :] = own.astype(BF16)
    for d in order:
        p_sends[d].wait_send()


def body(
    tokens, dec_tokens, norm_gain, w_query, w_key, w_value, w_out, head_gain, mix_lambda,
    ctx_keys, ctx_values, dec_keys, dec_values, dec_len, *, kv, tp,
):
    rows, width = tokens.shape
    drows = dec_tokens.shape[0]
    w = w_query.shape[2]
    heads = w // DH
    vwid = w_value.shape[1]
    ctx = ctx_keys.shape[1]
    slots = dec_keys.shape[2]
    cols = w_out.shape[1] // tp
    padded = rows + -(-drows // 16) * 16
    any_spec = pl.BlockSpec(memory_space=pltpu.HBM)
    vmem = pl.BlockSpec(memory_space=pltpu.VMEM)
    dma = pltpu.SemaphoreType.DMA
    V = pltpu.VMEM

    def hbm(x):
        return pltpu.with_memory_space_constraint(x, pltpu.HBM) if x.size > 1 else x

    out = pl.pallas_call(
        functools.partial(kernel, kv, tp),
        out_shape=jax.ShapeDtypeStruct((padded, cols), BF16),
        in_specs=[any_spec] * 8 + [pl.BlockSpec(memory_space=pl.ANY)] * 2 + [any_spec] * 4,
        out_specs=vmem,
        scratch_shapes=[
            pltpu.SMEM((heads,), F32), pltpu.SMEM((drows,), jnp.int32),
            V((rows, width), BF16), V((drows, width), BF16), V((1, width), F32),
            V((1, 2 * DH), F32),
            V((2, width, w), BF16), V((2, width, w), BF16), V((width, vwid), BF16),
            V((tp, vwid, cols), BF16),
            V((2, ctx, w), BF16), V((ctx, vwid), BF16),
            V((2, drows, slots, w), BF16), V((drows, slots, vwid), BF16),
            V((padded, width), BF16), V((heads, kv, rows, 2 * DH), BF16),
            V((2, LANES, w), BF16), V((LANES, vwid), BF16),
            V((heads, kv, 1, LANES), F32), V((heads, kv, 1, LANES), F32),
            V((heads, kv, rows, 4 * DH), BF16), V((heads, kv, rows, 4 * DH), BF16),
            V((tp, rows, cols), F32),
            V((tp, rows, cols), BF16), V((tp, rows, cols), BF16),
            V((tp, drows, cols), BF16), V((tp, drows, cols), BF16),
            dma((6,)), dma((heads * Q_PARTS,)), dma((K_PARTS,)), dma((V_PARTS,)), dma((tp,)),
            dma((2,)), dma((2,)),
            dma((heads, kv)), dma((heads, kv)), dma((heads, kv)), dma((heads, kv)),
            dma((heads, kv)), dma((heads, kv)),
            dma((tp,)), dma((tp,)), dma((tp,)), dma((tp,)),
        ],
        compiler_params=pltpu.CompilerParams(
            collective_id=0, has_side_effects=True, vmem_limit_bytes=48 * 1024 * 1024
        ),
    )(
        hbm(tokens), hbm(dec_tokens), hbm(norm_gain.reshape(1, width)), hbm(w_query),
        hbm(w_key), hbm(w_value), hbm(w_out), hbm(head_gain.reshape(1, 2 * DH)),
        hbm(mix_lambda), hbm(dec_len), hbm(ctx_keys), hbm(ctx_values), hbm(dec_keys),
        hbm(dec_values),
    )

    def split(src, piece_ref, dec_ref):
        piece_ref[...] = src[0:rows, :]
        dec_ref[...] = src[rows : rows + drows, :]

    return pl.pallas_call(
        split,
        out_shape=(
            jax.ShapeDtypeStruct((rows, cols), BF16),
            jax.ShapeDtypeStruct((drows, cols), BF16),
        ),
        in_specs=[vmem],
        out_specs=(vmem, vmem),
        compiler_params=pltpu.CompilerParams(vmem_limit_bytes=1024 * 1024),
    )(out)


def solution(mesh):
    in_specs = (
        P("kv", None),
        P("kv", None),
        P(),
        P(None, None, "tp"),
        P(None, None, "tp"),
        P(None, "tp"),
        P("tp", None),
        P(),
        P("tp"),
        P(None, "kv", "tp"),
        P("kv", "tp"),
        P(None, "kv", None, "tp"),
        P("kv", None, "tp"),
        P("kv"),
    )
    out_specs = (P("kv", "tp"), P("kv", "tp"))
    step = functools.partial(body, kv=mesh.shape["kv"], tp=mesh.shape["tp"])
    return jax.shard_map(step, mesh=mesh, in_specs=in_specs, out_specs=out_specs, check_vma=False)
```

time: 29.2 us -> 25.6 us (0.88)
  Pallas kernels: 27.8 us -> 24.2 us
    pallas_call x1, Pallas kernels: 26.3 us -> 23.6 us  [body(): pl.pallas_call(functools.partial(kernel, kv, tp), out_shape=jax.ShapeDtyp...]
    pallas_call x1, Pallas kernels: 1.46 us -> 0.62 us  [body(): pl.pallas_call(split, out_shape=(jax.ShapeDtypeStruct((rows, cols), BF16)...]
where the time goes in v1:
time: 25.6 us; the launch traced here: 25.5 us
  Pallas kernels  24.2 us (95%)
  between operations  1.29 us (5%)
    pallas_call x1, Pallas kernels, body(): pl.pallas_call(functools.partial(kernel, kv, tp), out_shape=jax.ShapeDtyp...  23.6 us
    pallas_call x1, Pallas kernels, body(): pl.pallas_call(split, out_shape=(jax.ShapeDtypeStruct((rows, cols), BF16)...  0.62 us

profile of v1, /device:TPU:0, one launch (start us, length us, event | category | flops | bytes accessed | tf_op | source)
XLA Modules:
  0.0 25.5 jit_solution(11117291208434754242)
XLA Ops:
  1.3 23.6 %shard_map.149.src = bf16[32,1024]{1,0:T(8,128)(2,1)S(1)} custom-call(bf16[16,4096]{1,0:T(8,128)(2,1)} %tokens.1, bf16[1,4096]{1,0:T(2,128)(2,1)} %dec_tokens.1, f32[1,4096]{1,0:T(1,128)} %bitcast.2, bf16[2,4096,256]{2,1,0:T(8,128)(2,1)} %w_query.1, bf16[2,4096,256]{2,1,0:T(8,128)(2,1)} %w_key.1, bf16[4096,512]{1,0:T(8,128)(2,1)} %w_value.1, ...), custom_call_target="tpu_custom_call" | custom-call | tf_op jit(solution)/shard_map/pallas_call | solution.py:431
  24.9 0.6 %shard_map.150 = (bf16[16,1024]{1,0:T(8,128)(2,1)}, bf16[1,1024]{1,0:T(2,128)(2,1)}) custom-call(bf16[32,1024]{1,0:T(8,128)(2,1)S(1)} %shard_map.149.src), custom_call_target="tpu_custom_call" | custom-call | tf_op jit(solution)/shard_map/pallas_call | solution.py:471

commit v2 on v1

--- a/solution.py
+++ b/solution.py
@@ -15,8 +15,10 @@
 BF16 = jnp.bfloat16
 LANES = 128
 C_EXP = DH ** (-0.5) * math.log2(math.e)
-Q_PARTS = 4
+Q_PARTS = 8
 K_PARTS = 2
+BLOCK = 64
+UNROLL = 4
 V_PARTS = 4
 
 
@@ -26,6 +28,10 @@
 
 def dot_nt(a, b):
     return lax.dot_general(a, b, (((1,), (1,)), ((), ())), preferred_element_type=F32)
+
+
+def piece_block(total):
+    return BLOCK if total % BLOCK == 0 else LANES
 
 
 def kernel(
@@ -35,7 +41,7 @@
     out,
     lam_s, len_s, tok_v, dtok_v, gain_v, hgain_v, wq_v, wk_v, wv_v, wo_v,
     ck_v, cv_v, dk_v, dv_v,
-    xs, q_all, kown, vown, st_send, st_recv, att_send, att_recv, po_acc, p_send, p_recv,
+    xs, q_all, kown, vown, st_send, st_recv, fac_v, att_send, att_recv, po_acc, p_send, p_recv,
     d_send, d_recv,
     sem_small, sem_q, sem_k, sem_v, sem_o, sem_c, sem_d,
     qs_sem, qr_sem, ss_sem, sr_sem, as_sem, ar_sem, ps_sem, pr_sem, ds_sem, dr_sem,
@@ -50,9 +56,10 @@
     slots = dec_keys.shape[2]
     total = rows * kv
     cols = w_out.shape[1] // tp
-    blocks = total // LANES
+    block = piece_block(total)
+    blocks = total // block
     padded = xs.shape[0]
-    per = LANES // rows
+    per = block // rows
 
     def tp_peer(d):
         chip = lax.rem(mt // 2 + d // 2, tp // 2)
@@ -83,15 +90,9 @@
     kstep = width // K_PARTS
     vstep = width // V_PARTS
     q_copies = []
-    for h in range(heads):
-        q_copies.append([])
-        for i in range(Q_PARTS):
-            sl = (slice(None), pl.ds(i * qstep, qstep), pl.ds(h * DH, DH))
-            q_copies[h].append(
-                pltpu.make_async_copy(
-                    w_query.at[sl], wq_v.at[sl], sem_q.at[h * Q_PARTS + i]
-                )
-            )
+    for i in range(Q_PARTS):
+        sl = (slice(None), pl.ds(i * qstep, qstep))
+        q_copies.append(pltpu.make_async_copy(w_query.at[sl], wq_v.at[sl], sem_q.at[i]))
     k_copies = []
     for i in range(K_PARTS):
         sl = (slice(None), pl.ds(i * kstep, kstep))
@@ -112,9 +113,8 @@
         wo_copies.append(
             pltpu.make_async_copy(w_out.at[:, pl.ds(start, cols)], wo_v.at[d], sem_o.at[d])
         )
-    for row in q_copies:
-        for c in row:
-            c.start()
+    for c in q_copies:
+        c.start()
 
     kown[...] = jnp.zeros_like(kown)
     vown[...] = jnp.zeros_like(vown)
@@ -137,37 +137,29 @@
             device_id=(lax.rem(me + d, kv), mt), device_id_type=MESH,
         )
 
+    def drain(ref, sem):
+        pltpu.make_async_copy(ref, ref, sem).wait()
+
     far_first = sorted(range(1, kv), key=lambda d: (-min(d, kv - d), d))
-    dec_qh = []
-    q_sends = []
-    for h in range(heads):
-        hs = slice(h * DH, (h + 1) * DH)
-        acc = None
-        for i in range(Q_PARTS):
-            q_copies[h][i].wait()
-            sl = slice(i * qstep, (i + 1) * qstep)
-            wt = jnp.concatenate([wq_v[0, sl, hs], wq_v[1, sl, hs]], axis=1)
-            term = dot(xs[:, sl], wt)
-            acc = term if acc is None else acc + term
-        qh = acc.astype(BF16)
-        q_all[h, me] = qh[0:rows]
-        dec_qh.append(qh[rows:])
-        if h == 0:
-            for c in k_copies + [ck_copy]:
-                c.start()
-        if h == heads - 1:
-            for c in v_copies + [cv_copy]:
-                c.start()
-        if h == 0:
-            pl.semaphore_wait(barrier, kv + tp - 2)
-        q_sends.append(
-            {
-                d: to_kv(q_all.at[h, me], q_all.at[h, me], qs_sem.at[h, d], qr_sem.at[h, d], d)
-                for d in far_first
-            }
-        )
-        for d in far_first:
-            q_sends[h][d].start()
+    for c in k_copies + [ck_copy]:
+        c.start()
+    acc = [None, None]
+    for i in range(Q_PARTS):
+        q_copies[i].wait()
+        sl = slice(i * qstep, (i + 1) * qstep)
+        for c in range(2):
+            term = dot(xs[:, sl], wq_v[c, sl, :])
+            acc[c] = term if acc[c] is None else acc[c] + term
+    dec_q = []
+    for c in range(2):
+        qc = acc[c].astype(BF16)
+        q_all[me, :, c * w : (c + 1) * w] = qc[0:rows]
+        dec_q.append(qc[rows:])
+    for c in v_copies + [cv_copy]:
+        c.start()
+    pl.semaphore_wait(barrier, kv + tp - 2)
+    for d in far_first:
+        to_kv(q_all.at[me], q_all.at[me], qs_sem, qr_sem.at[lax.div(me, per)], d).start()
 
     acc = [None, None]
     for i in range(K_PARTS):
@@ -196,23 +188,40 @@
 
     ck_copy.wait()
     cv_copy.wait()
-    nstat = 4
-
-    def head_block(h, b):
+    nstat = 4 * heads
+    most = LANES // rows
+
+    def wait_queries(b):
+        inside = lax.div(me, per) == b
+
+        @pl.when(inside)
+        def _():
+            drain(q_all.at[pl.ds(b * per, per - 1)], qr_sem.at[b])
+
+        @pl.when(jnp.logical_not(inside))
+        def _():
+            drain(q_all.at[pl.ds(b * per, per)], qr_sem.at[b])
+
+    def attend(b):
         slots_b = pl.ds(b * per, per)
-        qb = q_all[h, slots_b].reshape(LANES, 2 * DH)
-        pos = b * LANES + lax.broadcasted_iota(jnp.int32, (LANES, LANES), 0)
-        lane = lax.broadcasted_iota(jnp.int32, (LANES, LANES), 1)
+        qb = q_all[slots_b].reshape(block, 2 * w)
+        pos = b * block + lax.broadcasted_iota(jnp.int32, (block, LANES), 0)
+        lane = lax.broadcasted_iota(jnp.int32, (block, LANES), 1)
         ok = (lane < rows) & (lane + me * rows <= pos)
-        stats = jnp.zeros((LANES, LANES), F32)
-        hs = slice(h * DH, (h + 1) * DH)
-        hv = slice(h * vw, (h + 1) * vw)
+        ok = jnp.concatenate([ok] * heads, axis=0) if heads > 1 else ok
+        head_of = lax.broadcasted_iota(jnp.int32, (block, w), 1) // DH
+        stats = jnp.zeros((block, LANES), F32)
         far_p = []
         near_p = []
         for c in range(2):
-            q = qb[:, c * DH : (c + 1) * DH]
-            far = dot_nt(q, ck_v[c, :, hs])
-            near = dot_nt(q, kown[c, :, hs])
+            qc = qb[:, c * w : (c + 1) * w]
+            if heads > 1:
+                zero = jnp.zeros_like(qc)
+                qc = jnp.concatenate(
+                    [jnp.where(head_of == h, qc, zero) for h in range(heads)], axis=0
+                )
+            far = dot_nt(qc, ck_v[c])
+            near = dot_nt(qc, kown[c])
             near = jnp.where(ok, near, -jnp.inf)
             top = jnp.maximum(
                 jnp.max(far, axis=-1, keepdims=True), jnp.max(near, axis=-1, keepdims=True)
@@ -222,57 +231,63 @@
             tot = jnp.sum(ef, axis=-1, keepdims=True) + jnp.sum(en, axis=-1, keepdims=True)
             far_p.append(ef.astype(BF16))
             near_p.append(en.astype(BF16))
-            stats = jnp.where(lane == c, top, stats)
-            stats = jnp.where(lane == 2 + c, tot, stats)
-        for c in range(2):
-            att = dot(far_p[c], cv_v[:, hv]) + dot(near_p[c], vown[:, hv])
-            att_send[h, slots_b, :, c * vw : (c + 1) * vw] = att.astype(BF16).reshape(
-                per, rows, vw
+            for h in range(heads):
+                part = slice(h * block, (h + 1) * block)
+                stats = jnp.where(lane == 2 * h + c, top[part], stats)
+                stats = jnp.where(lane == 2 * heads + 2 * h + c, tot[part], stats)
+        for h in range(heads):
+            part = slice(h * block, (h + 1) * block)
+            hv = slice(h * vw, (h + 1) * vw)
+            att = dot(jnp.concatenate([p[part] for p in far_p], axis=0), cv_v[:, hv]) + dot(
+                jnp.concatenate([p[part] for p in near_p], axis=0), vown[:, hv]
             )
+            for c in range(2):
+                att_send[h, slots_b, :, c * vw : (c + 1) * vw] = (
+                    att[c * block : (c + 1) * block].astype(BF16).reshape(per, rows, vw)
+                )
+        if block < LANES:
+            stats = jnp.concatenate([stats, jnp.zeros((LANES - block, LANES), F32)], axis=0)
         by_row = jnp.transpose(stats)
-        lane8 = lax.broadcasted_iota(jnp.int32, (per, LANES), 1) // rows
-        packed = jnp.zeros((per, LANES), F32)
+        group_of = lax.broadcasted_iota(jnp.int32, (most, LANES), 1) // rows
+        packed = jnp.zeros((most, LANES), F32)
         for s in range(nstat):
-            line = jnp.broadcast_to(by_row[s : s + 1, :], (per, LANES))
+            line = jnp.broadcast_to(by_row[s : s + 1, :], (most, LANES))
             line = pltpu.roll(line, rows, 1, stride=rows, stride_axis=0)
             if s:
                 line = pltpu.roll(line, s * rows, 1)
-            packed = jnp.where(lane8 == s, line, packed)
+            packed = jnp.where(group_of == s, line, packed)
         for o in range(per):
-            st_send[h, b * per + o] = packed[per - 1 - o : per - o, :]
-
-    a_sends = []
-    st_sends = []
-    for h in range(heads):
-        for d in far_first:
-            q_sends[h][d].wait_recv()
-        if blocks == 1:
-            head_block(h, 0)
-        else:
-            pl.loop(0, blocks)(functools.partial(head_block, h))
-        st_recv[h, 0] = st_send[h, me]
-        for i in range(kv - 1):
-            peer = i + jnp.where(me <= i, 1, 0)
+            st_send[b * per + o] = packed[most - 1 - o : most - o, :]
+
+    def send_block(peers):
+        for peer in peers:
             d = lax.rem(peer - me + kv, kv)
-            to_kv(
-                st_send.at[h, peer], st_recv.at[h, d], ss_sem.at[h, d], sr_sem.at[h, d], d
-            ).start()
-        for i in range(kv - 1):
-            peer = i + jnp.where(me <= i, 1, 0)
+
+            @pl.when(peer != me)
+            def _(peer=peer, d=d):
+                to_kv(st_send.at[peer], st_recv.at[d], ss_sem, sr_sem, d).start()
+
+        for peer in peers:
             d = lax.rem(peer - me + kv, kv)
-            to_kv(
-                att_send.at[h, peer], att_recv.at[h, d], as_sem.at[h, d], ar_sem.at[h, d], d
-            ).start()
-        st_sends.append({})
-        a_sends.append({})
-        for d in range(1, kv):
-            peer = lax.rem(me + d, kv)
-            st_sends[h][d] = to_kv(
-                st_send.at[h, peer], st_recv.at[h, d], ss_sem.at[h, d], sr_sem.at[h, d], d
-            )
-            a_sends[h][d] = to_kv(
-                att_send.at[h, peer], att_recv.at[h, d], as_sem.at[h, d], ar_sem.at[h, d], d
-            )
+
+            @pl.when(peer != me)
+            def _(peer=peer, d=d):
+                for h in range(heads):
+                    to_kv(
+                        att_send.at[h, peer], att_recv.at[h, d], as_sem, ar_sem.at[h], d
+                    ).start()
+
+    if blocks <= UNROLL:
+        for b in range(blocks):
+            wait_queries(b)
+            attend(b)
+            send_block(range(b * per, (b + 1) * per))
+    else:
+        for b in range(blocks):
+            wait_queries(b)
+        pl.loop(0, blocks)(attend)
+        send_block(range(kv))
+    st_recv[0] = st_send[me]
 
     hgain = hgain_v[...]
     group = 16
@@ -287,9 +302,6 @@
     slot_id = lax.broadcasted_iota(jnp.int32, (group, slots), 1)
     vrow = lax.broadcasted_iota(jnp.int32, (group, heads * vw), 0)
     vcol = lax.broadcasted_iota(jnp.int32, (group, heads * vw), 1) // vw
-    dec_q = [
-        jnp.concatenate([q[:, c * DH : (c + 1) * DH] for q in dec_qh], axis=1) for c in range(2)
-    ]
     dec_att = []
     for r in range(drows):
         far_p = []
@@ -320,7 +332,7 @@
 
     def to_tp(src, dst, send, recv, d):
         return pltpu.make_async_remote_copy(
-            src_ref=src.at[d], dst_ref=dst.at[d], send_sem=send.at[d], recv_sem=recv.at[d],
+            src_ref=src.at[d], dst_ref=dst.at[d], send_sem=send, recv_sem=recv,
             device_id=(me, tp_peer(d)), device_id_type=MESH,
         )
 
@@ -349,26 +361,31 @@
 
     lane = lax.broadcasted_iota(jnp.int32, (1, LANES), 1)
     p_sends = {d: to_tp(p_send, p_recv, ps_sem, pr_sem, d) for d in order}
+    drain(st_recv.at[pl.ds(1, kv - 1)], sr_sem)
+    nmax = 2 * heads * rows
+    sts = st_recv[...].reshape(kv, LANES)
+    top = jnp.max(sts, axis=0, keepdims=True)
+    fac = jnp.exp2((sts - top) * C_EXP)
+    den = jnp.sum(fac * pltpu.roll(sts, LANES - nmax, 1), axis=0, keepdims=True)
+    den = jnp.where(lane < nmax, den, 1.0)
+    sign = jnp.ones((1, LANES), F32)
+    for h in range(heads):
+        sign = jnp.where(lane // rows == 2 * h + 1, -lam_s[h], sign)
+    fac = jnp.transpose(fac * (sign / den))
+    for i in range(2 * heads):
+        for d in range(kv):
+            fac_v[i, d] = jnp.broadcast_to(
+                fac[i * rows : (i + 1) * rows, d : d + 1], (rows, LANES)
+            )
     own = None
     for h in range(heads):
-        for d in range(1, kv):
-            st_sends[h][d].wait_recv()
-        sts = st_recv[h].reshape(kv, LANES)
-        top = jnp.max(sts, axis=0, keepdims=True)
-        fac = jnp.exp2((sts - top) * C_EXP)
-        den = jnp.sum(fac * pltpu.roll(sts, LANES - 2 * rows, 1), axis=0, keepdims=True)
-        den = jnp.where(lane < 2 * rows, den, 1.0)
-        part = jnp.where(lane < rows, 1.0, -lam_s[h]) / den
-        fac = jnp.transpose(fac * part)
+        drain(att_recv.at[h, pl.ds(1, kv - 1)], ar_sem.at[h])
         total_att = None
-        for d in [0] + far_first[::-1]:
-            if d == 0:
-                blk = att_send[h, me]
-            else:
-                a_sends[h][d].wait_recv()
-                blk = att_recv[h, d]
+        for d in range(kv):
+            blk = att_send[h, me] if d == 0 else att_recv[h, d]
             for c in range(2):
-                term = fac[c * rows : (c + 1) * rows, d : d + 1] * blk[
+                f = fac_v[2 * h + c, d]
+                term = jnp.concatenate([f] * (vw // LANES), axis=1) * blk[
                     :, c * vw : (c + 1) * vw
                 ].astype(F32)
                 total_att = term if total_att is None else total_att + term
@@ -382,29 +399,29 @@
                 po_acc[d] = term
             elif d > 0:
                 p_send[d] = term.astype(BF16)
-                p_sends[d].start()
             else:
                 own = term.astype(BF16).astype(F32)
+        if last:
+            for d in order:
+                p_sends[d].start()
+    drain(d_recv.at[pl.ds(1, tp - 1)], dr_sem)
     dsum = dec_own.astype(F32)
     for d in order:
-        d_sends[d].wait_recv()
         dsum = dsum + d_recv[d].astype(F32)
     out[rows:, :] = jnp.broadcast_to(dsum, (out.shape[0] - rows, cols)).astype(BF16) if (
         drows == 1
     ) else jnp.concatenate(
         [dsum, jnp.zeros((out.shape[0] - rows - drows, cols), F32)], axis=0
     ).astype(BF16)
-    for rem_sends in q_sends + st_sends + a_sends:
-        for d in range(1, kv):
-            rem_sends[d].wait_send()
+    drain(q_all.at[pl.ds(0, kv - 1)], qs_sem)
+    drain(st_send.at[pl.ds(0, kv - 1)], ss_sem)
+    drain(att_send.at[:, pl.ds(0, kv - 1)], as_sem)
+    drain(d_send.at[pl.ds(1, tp - 1)], ds_sem)
+    drain(p_send.at[pl.ds(1, tp - 1)], ps_sem)
+    drain(p_recv.at[pl.ds(1, tp - 1)], pr_sem)
     for d in order:
-        d_sends[d].wait_send()
-    for d in order[::-1]:
-        p_sends[d].wait_recv()
         own = own + p_recv[d].astype(F32)
     out[0:rows, :] = own.astype(BF16)
-    for d in order:
-        p_sends[d].wait_send()
 
 
 def body(
@@ -420,6 +437,7 @@
     slots = dec_keys.shape[2]
     cols = w_out.shape[1] // tp
     padded = rows + -(-drows // 16) * 16
+    blocks = rows * kv // piece_block(rows * kv)
     any_spec = pl.BlockSpec(memory_space=pltpu.HBM)
     vmem = pl.BlockSpec(memory_space=pltpu.VMEM)
     dma = pltpu.SemaphoreType.DMA
@@ -441,18 +459,18 @@
             V((tp, vwid, cols), BF16),
             V((2, ctx, w), BF16), V((ctx, vwid), BF16),
             V((2, drows, slots, w), BF16), V((drows, slots, vwid), BF16),
-            V((padded, width), BF16), V((heads, kv, rows, 2 * DH), BF16),
+            V((padded, width), BF16), V((kv, rows, 2 * w), BF16),
             V((2, LANES, w), BF16), V((LANES, vwid), BF16),
-            V((heads, kv, 1, LANES), F32), V((heads, kv, 1, LANES), F32),
+            V((kv, 1, LANES), F32), V((kv, 1, LANES), F32),
+            V((2 * heads, kv, rows, LANES), F32),
             V((heads, kv, rows, 4 * DH), BF16), V((heads, kv, rows, 4 * DH), BF16),
             V((tp, rows, cols), F32),
             V((tp, rows, cols), BF16), V((tp, rows, cols), BF16),
             V((tp, drows, cols), BF16), V((tp, drows, cols), BF16),
-            dma((6,)), dma((heads * Q_PARTS,)), dma((K_PARTS,)), dma((V_PARTS,)), dma((tp,)),
+            dma((6,)), dma((Q_PARTS,)), dma((K_PARTS,)), dma((V_PARTS,)), dma((tp,)),
             dma((2,)), dma((2,)),
-            dma((heads, kv)), dma((heads, kv)), dma((heads, kv)), dma((heads, kv)),
-            dma((heads, kv)), dma((heads, kv)),
-            dma((tp,)), dma((tp,)), dma((tp,)), dma((tp,)),
+            dma(()), dma((blocks,)), dma(()), dma(()), dma(()), dma((heads,)),
+            dma(()), dma(()), dma(()), dma(()),
         ],
         compiler_params=pltpu.CompilerParams(
             collective_id=0, has_side_effects=True, vmem_limit_bytes=48 * 1024 * 1024

time: 25.6 us -> 23.2 us (0.906)
  Pallas kernels: 24.2 us -> 21.8 us
    pallas_call x1, Pallas kernels: 23.6 us -> 21.2 us  [body(): pl.pallas_call(functools.partial(kernel, kv, tp), out_shape=jax.ShapeDtyp...]
where the time goes in v2:
time: 23.2 us; the launch traced here: 23.1 us
  Pallas kernels  21.8 us (94%)
  between operations  1.29 us (6%)
    pallas_call x1, Pallas kernels, body(): pl.pallas_call(functools.partial(kernel, kv, tp), out_shape=jax.ShapeDtyp...  21.2 us
    pallas_call x1, Pallas kernels, body(): pl.pallas_call(split, out_shape=(jax.ShapeDtypeStruct((rows, cols), BF16)...  0.62 us

profile of v2, /device:TPU:0, one launch (start us, length us, event | category | flops | bytes accessed | tf_op | source)
XLA Modules:
  0.0 23.1 jit_solution(5084852177622555578)
XLA Ops:
  1.3 21.2 %shard_map.149.src = bf16[32,1024]{1,0:T(8,128)(2,1)S(1)} custom-call(bf16[16,4096]{1,0:T(8,128)(2,1)} %tokens.1, bf16[1,4096]{1,0:T(2,128)(2,1)} %dec_tokens.1, f32[1,4096]{1,0:T(1,128)} %bitcast.2, bf16[2,4096,256]{2,1,0:T(8,128)(2,1)} %w_query.1, bf16[2,4096,256]{2,1,0:T(8,128)(2,1)} %w_key.1, bf16[4096,512]{1,0:T(8,128)(2,1)} %w_value.1, ...), custom_call_target="tpu_custom_call" | custom-call | tf_op jit(solution)/shard_map/pallas_call | solution.py:449
  22.5 0.6 %shard_map.150 = (bf16[16,1024]{1,0:T(8,128)(2,1)}, bf16[1,1024]{1,0:T(2,128)(2,1)}) custom-call(bf16[32,1024]{1,0:T(8,128)(2,1)S(1)} %shard_map.149.src), custom_call_target="tpu_custom_call" | custom-call | tf_op jit(solution)/shard_map/pallas_call | solution.py:489

commit v3 on v2

--- a/solution.py
+++ b/solution.py
@@ -18,8 +18,9 @@
 Q_PARTS = 8
 K_PARTS = 2
 BLOCK = 64
-UNROLL = 4
-V_PARTS = 4
+UNROLL = 8
+UNIT = 2
+V_PARTS = 2
 
 
 def dot(a, b):
@@ -41,7 +42,7 @@
     out,
     lam_s, len_s, tok_v, dtok_v, gain_v, hgain_v, wq_v, wk_v, wv_v, wo_v,
     ck_v, cv_v, dk_v, dv_v,
-    xs, q_all, kown, vown, st_send, st_recv, fac_v, att_send, att_recv, po_acc, p_send, p_recv,
+    kt_v, kn_v, xs, q_all, kown, vown, st_send, st_recv, fac_v, att_send, att_recv, p_send, p_recv,
     d_send, d_recv,
     sem_small, sem_q, sem_k, sem_v, sem_o, sem_c, sem_d,
     qs_sem, qr_sem, ss_sem, sr_sem, as_sem, ar_sem, ps_sem, pr_sem, ds_sem, dr_sem,
@@ -111,15 +112,15 @@
     for d in range(tp):
         start = pl.multiple_of(tp_peer(d) * cols, LANES)
         wo_copies.append(
-            pltpu.make_async_copy(w_out.at[:, pl.ds(start, cols)], wo_v.at[d], sem_o.at[d])
+            pltpu.make_async_copy(w_out.at[:, pl.ds(start, cols)], wo_v.at[d], sem_o)
         )
     for c in q_copies:
-        c.start()
+        c.start(priority=1)
 
     kown[...] = jnp.zeros_like(kown)
     vown[...] = jnp.zeros_like(vown)
     xs[rows:, :] = jnp.zeros((padded - rows, width), BF16)
-    for c in small:
+    for c in small[:3]:
         c.wait()
     gain = gain_v[...]
 
@@ -134,15 +135,19 @@
     def to_kv(src, dst, send, recv, d):
         return pltpu.make_async_remote_copy(
             src_ref=src, dst_ref=dst, send_sem=send, recv_sem=recv,
-            device_id=(lax.rem(me + d, kv), mt), device_id_type=MESH,
+            device_id=(lax.rem(me + d + kv, kv), mt), device_id_type=MESH,
         )
 
     def drain(ref, sem):
         pltpu.make_async_copy(ref, ref, sem).wait()
 
-    far_first = sorted(range(1, kv), key=lambda d: (-min(d, kv - d), d))
+    def far_peer(i):
+        down = kv - 1 - i - jnp.where(kv - 1 - i <= me, 1, 0)
+        up = i + jnp.where(i >= me, 1, 0)
+        return jnp.where(2 * me < kv, down, up)
+
     for c in k_copies + [ck_copy]:
-        c.start()
+        c.start(priority=1)
     acc = [None, None]
     for i in range(Q_PARTS):
         q_copies[i].wait()
@@ -156,10 +161,18 @@
         q_all[me, :, c * w : (c + 1) * w] = qc[0:rows]
         dec_q.append(qc[rows:])
     for c in v_copies + [cv_copy]:
-        c.start()
+        c.start(priority=1)
     pl.semaphore_wait(barrier, kv + tp - 2)
-    for d in far_first:
-        to_kv(q_all.at[me], q_all.at[me], qs_sem, qr_sem.at[lax.div(me, per)], d).start()
+    for i in range(kv - 1):
+        ring = sorted(range(1, kv), key=lambda d: (-min(d, kv - d), d))[i]
+        half = kv // 2
+        if i < half:
+            up_first = half + i - me
+        else:
+            near = i - half
+            up_first = near + jnp.where(near >= me, 1, 0) - me
+        d = jnp.where(me < half, up_first, ring)
+        to_kv(q_all.at[me], q_all.at[me], qs_sem, qr_sem.at[lax.div(me, UNIT)], d).start()
 
     acc = [None, None]
     for i in range(K_PARTS):
@@ -173,8 +186,12 @@
         kc = acc[c].astype(BF16)
         kown[c, 0:rows, :] = kc[0:rows]
         dec_k.append(kc[rows:])
+    ck_copy.wait()
+    for c in range(2):
+        kt_v[c] = jnp.transpose(ck_v[c])
+        kn_v[c] = jnp.transpose(kown[c])
     for c in [dk_copy, dv_copy]:
-        c.start()
+        c.start(priority=1)
     acc = None
     for i in range(V_PARTS):
         v_copies[i].wait()
@@ -184,28 +201,28 @@
     vown[0:rows, :] = vc[0:rows]
     dec_v = vc[rows:]
     for c in wo_copies:
-        c.start()
-
-    ck_copy.wait()
+        c.start(priority=1)
+
     cv_copy.wait()
     nstat = 4 * heads
     most = LANES // rows
 
-    def wait_queries(b):
-        inside = lax.div(me, per) == b
+    def wait_queries(u):
+        inside = lax.div(me, UNIT) == u
 
         @pl.when(inside)
         def _():
-            drain(q_all.at[pl.ds(b * per, per - 1)], qr_sem.at[b])
+            drain(q_all.at[pl.ds(u * UNIT, UNIT - 1)], qr_sem.at[u])
 
         @pl.when(jnp.logical_not(inside))
         def _():
-            drain(q_all.at[pl.ds(b * per, per)], qr_sem.at[b])
-
-    def attend(b):
-        slots_b = pl.ds(b * per, per)
+            drain(q_all.at[pl.ds(u * UNIT, UNIT)], qr_sem.at[u])
+
+    def attend(first, per):
+        block = per * rows
+        slots_b = pl.ds(first, per)
         qb = q_all[slots_b].reshape(block, 2 * w)
-        pos = b * block + lax.broadcasted_iota(jnp.int32, (block, LANES), 0)
+        pos = first * rows + lax.broadcasted_iota(jnp.int32, (block, LANES), 0)
         lane = lax.broadcasted_iota(jnp.int32, (block, LANES), 1)
         ok = (lane < rows) & (lane + me * rows <= pos)
         ok = jnp.concatenate([ok] * heads, axis=0) if heads > 1 else ok
@@ -220,8 +237,8 @@
                 qc = jnp.concatenate(
                     [jnp.where(head_of == h, qc, zero) for h in range(heads)], axis=0
                 )
-            far = dot_nt(qc, ck_v[c])
-            near = dot_nt(qc, kown[c])
+            far = dot(qc, kt_v[c])
+            near = dot(qc, kn_v[c])
             near = jnp.where(ok, near, -jnp.inf)
             top = jnp.maximum(
                 jnp.max(far, axis=-1, keepdims=True), jnp.max(near, axis=-1, keepdims=True)
@@ -257,7 +274,7 @@
                 line = pltpu.roll(line, s * rows, 1)
             packed = jnp.where(group_of == s, line, packed)
         for o in range(per):
-            st_send[b * per + o] = packed[most - 1 - o : most - o, :]
+            st_send[first + o] = packed[most - 1 - o : most - o, :]
 
     def send_block(peers):
         for peer in peers:
@@ -274,21 +291,30 @@
             def _(peer=peer, d=d):
                 for h in range(heads):
                     to_kv(
-                        att_send.at[h, peer], att_recv.at[h, d], as_sem, ar_sem.at[h], d
+                        att_send.at[h, peer], att_recv.at[h, d], as_sem, ar_sem, d
                     ).start()
 
-    if blocks <= UNROLL:
-        for b in range(blocks):
-            wait_queries(b)
-            attend(b)
-            send_block(range(b * per, (b + 1) * per))
+    units = kv // UNIT
+    if kv <= UNROLL:
+        quarter, half = kv // 4, kv // 2
+        for first, count, peers in (
+            (0, quarter, range(quarter)),
+            (quarter, half - quarter, range(quarter, half)),
+            (half, kv - half, range(half, kv)),
+        ):
+            for u in range(first // UNIT, (first + count) // UNIT):
+                wait_queries(u)
+            attend(first, count)
+            send_block(peers)
     else:
-        for b in range(blocks):
-            wait_queries(b)
-        pl.loop(0, blocks)(attend)
+        for u in range(units):
+            wait_queries(u)
+        pl.loop(0, blocks)(lambda b: attend(b * per, per))
         send_block(range(kv))
     st_recv[0] = st_send[me]
 
+    for c in small[3:]:
+        c.wait()
     hgain = hgain_v[...]
     group = 16
     hrow = lax.broadcasted_iota(jnp.int32, (group, w), 0)
@@ -342,9 +368,8 @@
     dec_rows = jnp.concatenate(dec_att, axis=0) if drows > 1 else dec_att[0]
     dec_rows = dec_rows if drows > 1 else jnp.broadcast_to(dec_rows, (group, heads * vw))
     dec_ho = [head_norm(dec_rows[:, h * vw : (h + 1) * vw]) for h in range(heads)]
-    for c in wo_copies:
-        c.wait()
-    order = list(range(tp - 1, 0, -1))
+    drain(wo_v, sem_o)
+    order = sorted(range(1, tp), key=lambda d: (d < 2, d))
 
     def dec_project(d):
         acc = None
@@ -377,9 +402,9 @@
             fac_v[i, d] = jnp.broadcast_to(
                 fac[i * rows : (i + 1) * rows, d : d + 1], (rows, LANES)
             )
-    own = None
+    drain(att_recv.at[:, pl.ds(1, kv - 1)], ar_sem)
+    ho = []
     for h in range(heads):
-        drain(att_recv.at[h, pl.ds(1, kv - 1)], ar_sem.at[h])
         total_att = None
         for d in range(kv):
             blk = att_send[h, me] if d == 0 else att_recv[h, d]
@@ -389,20 +414,17 @@
                     :, c * vw : (c + 1) * vw
                 ].astype(F32)
                 total_att = term if total_att is None else total_att + term
-        ho = head_norm(total_att)
-        last = h == heads - 1
-        for d in order + [0]:
-            term = out_part(ho, d, h)
-            if h > 0:
-                term = term + po_acc[d]
-            if not last:
-                po_acc[d] = term
-            elif d > 0:
-                p_send[d] = term.astype(BF16)
+        ho.append(head_norm(total_att))
+    ho = jnp.concatenate(ho, axis=1) if heads > 1 else ho[0]
+    for group_d in (order[:1], order[1:] + [0]):
+        for d in group_d:
+            term = dot(ho, wo_v[d]).astype(BF16)
+            if d > 0:
+                p_send[d] = term
             else:
-                own = term.astype(BF16).astype(F32)
-        if last:
-            for d in order:
+                own = term.astype(F32)
+        for d in group_d:
+            if d > 0:
                 p_sends[d].start()
     drain(d_recv.at[pl.ds(1, tp - 1)], dr_sem)
     dsum = dec_own.astype(F32)
@@ -437,7 +459,6 @@
     slots = dec_keys.shape[2]
     cols = w_out.shape[1] // tp
     padded = rows + -(-drows // 16) * 16
-    blocks = rows * kv // piece_block(rows * kv)
     any_spec = pl.BlockSpec(memory_space=pltpu.HBM)
     vmem = pl.BlockSpec(memory_space=pltpu.VMEM)
     dma = pltpu.SemaphoreType.DMA
@@ -459,17 +480,17 @@
             V((tp, vwid, cols), BF16),
             V((2, ctx, w), BF16), V((ctx, vwid), BF16),
             V((2, drows, slots, w), BF16), V((drows, slots, vwid), BF16),
+            V((2, w, ctx), BF16), V((2, w, LANES), BF16),
             V((padded, width), BF16), V((kv, rows, 2 * w), BF16),
             V((2, LANES, w), BF16), V((LANES, vwid), BF16),
             V((kv, 1, LANES), F32), V((kv, 1, LANES), F32),
             V((2 * heads, kv, rows, LANES), F32),
             V((heads, kv, rows, 4 * DH), BF16), V((heads, kv, rows, 4 * DH), BF16),
-            V((tp, rows, cols), F32),
             V((tp, rows, cols), BF16), V((tp, rows, cols), BF16),
             V((tp, drows, cols), BF16), V((tp, drows, cols), BF16),
-            dma((6,)), dma((Q_PARTS,)), dma((K_PARTS,)), dma((V_PARTS,)), dma((tp,)),
+            dma((6,)), dma((Q_PARTS,)), dma((K_PARTS,)), dma((V_PARTS,)), dma(()),
             dma((2,)), dma((2,)),
-            dma(()), dma((blocks,)), dma(()), dma(()), dma(()), dma((heads,)),
+            dma(()), dma((kv // UNIT,)), dma(()), dma(()), dma(()), dma(()),
             dma(()), dma(()), dma(()), dma(()),
         ],
         compiler_params=pltpu.CompilerParams(

time: 23.2 us -> 22.4 us (0.966)
  Pallas kernels: 21.8 us -> 20.9 us
    pallas_call x1, Pallas kernels: 21.2 us -> 20.3 us  [body(): pl.pallas_call(functools.partial(kernel, kv, tp), out_shape=jax.ShapeDtyp...]
where the time goes in v3:
time: 22.4 us; the launch traced here: 22.2 us
  Pallas kernels  20.9 us (93%)
  between operations  1.29 us (6%)
    pallas_call x1, Pallas kernels, body(): pl.pallas_call(functools.partial(kernel, kv, tp), out_shape=jax.ShapeDtyp...  20.3 us
    pallas_call x1, Pallas kernels, body(): pl.pallas_call(split, out_shape=(jax.ShapeDtypeStruct((rows, cols), BF16)...  0.62 us

profile of v3, /device:TPU:0, one launch (start us, length us, event | category | flops | bytes accessed | tf_op | source)
XLA Modules:
  0.0 22.2 jit_solution(1635735039523994131)
XLA Ops:
  1.3 20.3 %shard_map.149.src = bf16[32,1024]{1,0:T(8,128)(2,1)S(1)} custom-call(bf16[16,4096]{1,0:T(8,128)(2,1)} %tokens.1, bf16[1,4096]{1,0:T(2,128)(2,1)} %dec_tokens.1, f32[1,4096]{1,0:T(1,128)} %bitcast.2, bf16[2,4096,256]{2,1,0:T(8,128)(2,1)} %w_query.1, bf16[2,4096,256]{2,1,0:T(8,128)(2,1)} %w_key.1, bf16[4096,512]{1,0:T(8,128)(2,1)} %w_value.1, ...), custom_call_target="tpu_custom_call" | custom-call | tf_op jit(solution)/shard_map/pallas_call | solution.py:470
  21.6 0.6 %shard_map.150 = (bf16[16,1024]{1,0:T(8,128)(2,1)}, bf16[1,1024]{1,0:T(2,128)(2,1)}) custom-call(bf16[32,1024]{1,0:T(8,128)(2,1)S(1)} %shard_map.149.src), custom_call_target="tpu_custom_call" | custom-call | tf_op jit(solution)/shard_map/pallas_call | solution.py:510

commit v4 on v3

--- a/solution.py
+++ b/solution.py
@@ -141,11 +141,6 @@
     def drain(ref, sem):
         pltpu.make_async_copy(ref, ref, sem).wait()
 
-    def far_peer(i):
-        down = kv - 1 - i - jnp.where(kv - 1 - i <= me, 1, 0)
-        up = i + jnp.where(i >= me, 1, 0)
-        return jnp.where(2 * me < kv, down, up)
-
     for c in k_copies + [ck_copy]:
         c.start(priority=1)
     acc = [None, None]
@@ -167,7 +162,7 @@
         ring = sorted(range(1, kv), key=lambda d: (-min(d, kv - d), d))[i]
         half = kv // 2
         if i < half:
-            up_first = half + i - me
+            up_first = half + (i ^ 1 if half % 2 == 0 else i) - me
         else:
             near = i - half
             up_first = near + jnp.where(near >= me, 1, 0) - me
@@ -295,7 +290,7 @@
                     ).start()
 
     units = kv // UNIT
-    if kv <= UNROLL:
+    if kv <= UNROLL and kv % (4 * UNIT) == 0:
         quarter, half = kv // 4, kv // 2
         for first, count, peers in (
             (0, quarter, range(quarter)),
@@ -305,7 +300,18 @@
             for u in range(first // UNIT, (first + count) // UNIT):
                 wait_queries(u)
             attend(first, count)
-            send_block(peers)
+            late = 4 * me >= 3 * kv
+            if first == quarter:
+                pl.when(lax.rem(mt, 2) == 0)(functools.partial(send_block, range(1, quarter)))
+                pl.when(jnp.logical_not(late))(functools.partial(send_block, peers))
+            else:
+                if first == half:
+                    pl.when(late)(functools.partial(send_block, range(quarter, half)))
+                    send_block(peers[::2])
+                    send_block(peers[1::2])
+                else:
+                    send_block(peers[:1])
+                    pl.when(lax.rem(mt, 2) == 1)(functools.partial(send_block, peers[1:]))
     else:
         for u in range(units):
             wait_queries(u)

time: 22.4 us -> 22 us (0.982)
  Pallas kernels: 20.9 us -> 20.6 us
    pallas_call x1, Pallas kernels: 20.3 us -> 20 us  [body(): pl.pallas_call(functools.partial(kernel, kv, tp), out_shape=jax.ShapeDtyp...]
where the time goes in v4:
time: 22 us; the launch traced here: 21.9 us
  Pallas kernels  20.6 us (94%)
  between operations  1.29 us (6%)
    pallas_call x1, Pallas kernels, body(): pl.pallas_call(functools.partial(kernel, kv, tp), out_shape=jax.ShapeDtyp...  20 us
    pallas_call x1, Pallas kernels, body(): pl.pallas_call(split, out_shape=(jax.ShapeDtypeStruct((rows, cols), BF16)...  0.62 us

profile of v4, /device:TPU:0, one launch (start us, length us, event | category | flops | bytes accessed | tf_op | source)
XLA Modules:
  0.0 21.9 jit_solution(2531616683433321546)
XLA Ops:
  1.3 20.0 %shard_map.149.src = bf16[32,1024]{1,0:T(8,128)(2,1)S(1)} custom-call(bf16[16,4096]{1,0:T(8,128)(2,1)} %tokens.1, bf16[1,4096]{1,0:T(2,128)(2,1)} %dec_tokens.1, f32[1,4096]{1,0:T(1,128)} %bitcast.2, bf16[2,4096,256]{2,1,0:T(8,128)(2,1)} %w_query.1, bf16[2,4096,256]{2,1,0:T(8,128)(2,1)} %w_key.1, bf16[4096,512]{1,0:T(8,128)(2,1)} %w_value.1, ...), custom_call_target="tpu_custom_call" | custom-call | tf_op jit(solution)/shard_map/pallas_call | solution.py:476
  21.2 0.6 %shard_map.150 = (bf16[16,1024]{1,0:T(8,128)(2,1)}, bf16[1,1024]{1,0:T(2,128)(2,1)}) custom-call(bf16[32,1024]{1,0:T(8,128)(2,1)S(1)} %shard_map.149.src), custom_call_target="tpu_custom_call" | custom-call | tf_op jit(solution)/shard_map/pallas_call | solution.py:516

commit v5 on v4

--- a/solution.py
+++ b/solution.py
@@ -166,7 +166,11 @@
         else:
             near = i - half
             up_first = near + jnp.where(near >= me, 1, 0) - me
-        d = jnp.where(me < half, up_first, ring)
+        if i < half:
+            down_first = half - 1 - i - me
+        else:
+            down_first = i + jnp.where(i >= me, 1, 0) - me
+        d = jnp.where(me < half, up_first, down_first)
         to_kv(q_all.at[me], q_all.at[me], qs_sem, qr_sem.at[lax.div(me, UNIT)], d).start()
 
     acc = [None, None]

time: 22 us -> 22 us (level)
  no operation moved by 1% of the time
where the time goes in v5:
time: 22 us; the launch traced here: 21.9 us
  Pallas kernels  20.6 us (94%)
  between operations  1.29 us (6%)
    pallas_call x1, Pallas kernels, body(): pl.pallas_call(functools.partial(kernel, kv, tp), out_shape=jax.ShapeDtyp...  20 us
    pallas_call x1, Pallas kernels, body(): pl.pallas_call(split, out_shape=(jax.ShapeDtypeStruct((rows, cols), BF16)...  0.62 us

profile of v5, /device:TPU:0, one launch (start us, length us, event | category | flops | bytes accessed | tf_op | source)
XLA Modules:
  0.0 21.9 jit_solution(3904546086675947524)
XLA Ops:
  1.3 20.0 %shard_map.149.src = bf16[32,1024]{1,0:T(8,128)(2,1)S(1)} custom-call(bf16[16,4096]{1,0:T(8,128)(2,1)} %tokens.1, bf16[1,4096]{1,0:T(2,128)(2,1)} %dec_tokens.1, f32[1,4096]{1,0:T(1,128)} %bitcast.2, bf16[2,4096,256]{2,1,0:T(8,128)(2,1)} %w_query.1, bf16[2,4096,256]{2,1,0:T(8,128)(2,1)} %w_key.1, bf16[4096,512]{1,0:T(8,128)(2,1)} %w_value.1, ...), custom_call_target="tpu_custom_call" | custom-call | tf_op jit(solution)/shard_map/pallas_call | solution.py:480
  21.2 0.6 %shard_map.150 = (bf16[16,1024]{1,0:T(8,128)(2,1)}, bf16[1,1024]{1,0:T(2,128)(2,1)}) custom-call(bf16[32,1024]{1,0:T(8,128)(2,1)S(1)} %shard_map.149.src), custom_call_target="tpu_custom_call" | custom-call | tf_op jit(solution)/shard_map/pallas_call | solution.py:520
